TPU v7x, 32 devices: a whole 2x2x4 slice. The times are simulated.
32 devices in a mesh: gr: 2 (over x), fs: 8 (over z, y), tp: 2 (over core).
Axes of the slice: x: 2, y: 2, z: 4, core: 2. Of those that a mesh axis runs over, the one named last changes fastest.
Arguments:
- tokens: bfloat16 [4096, 2048], P(('gr', 'fs', 'tp')), may hold values from -6 to 6
- routes: int32 [4096, 8], P(('gr', 'fs', 'tp')), may hold values from 0 to 15, all different within a row; in each aligned block of 128 rows (0 to 127, 128 to 255, ...) at most 96 rows name the same one
- route_weights: float32 [4096, 8], P(('gr', 'fs', 'tp')), may hold values from 0.1 to 0.6
- norm_gain: float32 [2048], P(('gr', 'tp')), may hold values from 0.1 to 1.9
- gate_trained: float32 [16, 384, 2048], P(None, 'fs', ('gr', 'tp')), may hold values from -0.125 to 0.125
- up_trained: float32 [16, 384, 2048], P(None, 'fs', ('gr', 'tp')), may hold values from -0.125 to 0.125
- down_trained: float32 [16, 384, 2048], P(None, 'fs', ('gr', 'tp')), may hold values from -0.3125 to 0.3125
- shared_gate_trained: float32 [512, 2048], P('fs', ('gr', 'tp')), may hold values from -0.125 to 0.125
- shared_up_trained: float32 [512, 2048], P('fs', ('gr', 'tp')), may hold values from -0.125 to 0.125
- shared_down_trained: float32 [512, 2048], P('fs', ('gr', 'tp')), may hold values from -0.25 to 0.25
Outputs:
- combined: bfloat16 [4096, 2048], P(('gr', 'fs', 'tp'))
- expert_gate: bfloat16 [16, 384, 2048], P(('fs', 'tp'))
- expert_up: bfloat16 [16, 384, 2048], P(('fs', 'tp'))
- expert_down: bfloat16 [16, 384, 2048], P(('fs', 'tp'))
- shared_gate: bfloat16 [512, 2048], P('fs')
- shared_up: bfloat16 [512, 2048], P('fs')
- shared_down: bfloat16 [512, 2048], P('fs')
Inputs may be any that keep to these rules, and one draw needn't show every extreme that they name: `routes`: each row names 8 different experts. Among the rows of one device no expert is named more than 96 times, and that many is reached in every draw.
All inputs are finite; a program needn't handle non-finite values.
Results may differ from a plain program's by a relative error of at most 0.0084.
Values may be sent and summed in bfloat16 or wider, within the bound.
A program may use at most 128 MiB of HBM per device.

v0:
```python
import jax
import jax.numpy as jnp
from jax import lax
from jax.sharding import PartitionSpec as P

epsilon = 1e-06


def contract_rows(inputs, matrix):
    return lax.dot_general(
        inputs, matrix, (((1,), (1,)), ((), ())), preferred_element_type=jnp.float32
    )


def swiglu_rows(inputs, gate_matrix, up_matrix, down_matrix):
    hidden = (
        jax.nn.silu(contract_rows(inputs, gate_matrix)) * contract_rows(inputs, up_matrix)
    ).astype(jnp.bfloat16)
    return jnp.dot(hidden, down_matrix, preferred_element_type=jnp.float32)


def body(
    tokens,
    routes,
    route_weights,
    norm_gain,
    gate_trained,
    up_trained,
    down_trained,
    shared_gate_trained,
    shared_up_trained,
    shared_down_trained,
):
    gain_row = norm_gain[None, None, :]
    stacked = jnp.stack(
        [gate_trained * gain_row, up_trained * gain_row, down_trained], axis=1
    ).astype(jnp.bfloat16)
    halves = lax.all_to_all(
        lax.all_to_all(stacked[:, :, :, None, :], "fs", split_axis=0, concat_axis=2, tiled=True),
        "tp",
        split_axis=0,
        concat_axis=3,
        tiled=True,
    )
    owned = lax.all_gather(halves[:, :, :, None], "gr", axis=3, tiled=True)
    owned = owned.reshape(owned.shape[0], 3, owned.shape[2], -1)
    expert_gate = owned[:, 0]
    expert_up = owned[:, 1]
    expert_down = owned[:, 2]
    shared_gain = norm_gain[None, :]
    shared_stack = jnp.stack(
        [shared_gate_trained * shared_gain, shared_up_trained * shared_gain, shared_down_trained],
        axis=0,
    ).astype(jnp.bfloat16)
    shared_whole = lax.all_gather(shared_stack, ("gr", "tp"), axis=2, tiled=True)
    shared_gate = shared_whole[0]
    shared_up = shared_whole[1]
    shared_down = shared_whole[2]
    values = tokens.astype(jnp.float32)
    normed = (
        values * lax.rsqrt(jnp.mean(values * values, axis=1, keepdims=True) + epsilon)
    ).astype(jnp.bfloat16)
    row_count, features = normed.shape
    per_token = routes.shape[1]
    shared_out = swiglu_rows(
        normed,
        lax.all_gather(shared_gate, "fs", axis=0, tiled=True),
        lax.all_gather(shared_up, "fs", axis=0, tiled=True),
        lax.all_gather(shared_down, "fs", axis=0, tiled=True),
    )
    experts = lax.axis_size("fs") * lax.axis_size("tp")
    capacity = max(2, 3 * row_count * per_token // (2 * experts))
    chosen = routes.reshape(-1)
    onehot = (chosen[:, None] == jnp.arange(experts, dtype=jnp.int32)[None, :]).astype(jnp.int32)
    position = jnp.sum((jnp.cumsum(onehot, axis=0) - onehot) * onehot, axis=1)
    target = chosen * capacity + position
    source = (
        jnp.full((experts * capacity,), row_count, jnp.int32)
        .at[target]
        .set(jnp.arange(row_count * per_token, dtype=jnp.int32) // per_token)
    )
    padded = jnp.concatenate([normed, jnp.zeros((1, features), jnp.bfloat16)], axis=0)
    outgoing = padded[source].reshape(experts, capacity, features)
    arrived = lax.all_to_all(outgoing, ("fs", "tp"), split_axis=0, concat_axis=0, tiled=True)
    item_count = arrived.shape[1]
    result = swiglu_rows(
        arrived.reshape(-1, features), expert_gate[0], expert_up[0], expert_down[0]
    )
    result = result.astype(jnp.bfloat16).reshape(experts, item_count, features)
    returned = lax.all_to_all(result, ("fs", "tp"), split_axis=0, concat_axis=0, tiled=True)
    picked = returned.reshape(experts * capacity, features)[target].astype(jnp.float32)
    picked = picked.reshape(row_count, per_token, features)
    routed = jnp.sum(picked * route_weights[:, :, None], axis=1)
    combined = (routed + shared_out).astype(jnp.bfloat16)
    return (combined, expert_gate, expert_up, expert_down, shared_gate, shared_up, shared_down)


def solution(mesh):
    in_specs = (
        P(("gr", "fs", "tp"), None),
        P(("gr", "fs", "tp"), None),
        P(("gr", "fs", "tp"), None),
        P(("gr", "tp")),
        P(None, "fs", ("gr", "tp")),
        P(None, "fs", ("gr", "tp")),
        P(None, "fs", ("gr", "tp")),
        P("fs", ("gr", "tp")),
        P("fs", ("gr", "tp")),
        P("fs", ("gr", "tp")),
    )
    out_specs = (
        P(("gr", "fs", "tp"), None),
        P(("fs", "tp"), None, None),
        P(("fs", "tp"), None, None),
        P(("fs", "tp"), None, None),
        P("fs", None),
        P("fs", None),
        P("fs", None),
    )
    return jax.shard_map(body, mesh=mesh, in_specs=in_specs, out_specs=out_specs, check_vma=False)
```

profile of v0, /device:TPU:0, one launch (start us, length us, event | category | flops | bytes accessed | tf_op | source)
XLA Modules:
  0.0 506.6 jit_solution(6187070013755928364)
XLA Ops:
  8.0 0.0 copy-start.6
  8.0 0.0 copy-start.1
  8.0 1.6 convert_bitcast_fusion
  9.7 0.0 copy-done.6
  9.7 0.2 copy-done.1
  9.9 1.9 fusion.27
  11.8 1.7 pad_maximum_fusion
  13.5 0.0 copy-start.5
  13.5 0.0 copy-start
  13.5 7.4 %all-to-all-start.1 = ((bf16[16,3,48,1,512]{4,2,3,1,0:T(8,128)(2,1)}), bf16[16,3,48,1,512]{4,2,3,1,0:T(8,128)(2,1)S(1)}, u32[]{:S(2)}, u32[]{:S(2)}) async-start(bf16[16,3,48,1,512]{4,2,3,1,0:T(8,128)(2,1)} %pad_maximum_fusion), calls=%async_computation.1 | async-start | bytes 4718592 | tf_op jit(solution)/shard_map/all_to_all | solution.py:39
  20.9 0.0 copy-done.5
  20.9 0.1 copy.38
  21.0 0.1 eq.29
  21.1 0.1 eq.25
  21.2 4.5 reduce-window.6
  25.8 0.1 slice.36
  25.8 0.1 copy.40
  26.0 0.1 copy.41
  26.1 0.1 copy.37
  26.2 0.1 mul.85
  26.3 0.0 copy-done
  26.3 0.2 fusion.23
  26.5 0.2 fusion.24
  26.7 0.1 broadcast_add_fusion
  26.9 4.3 scatter_custom_fusion
  31.2 7.1 %gather_fusion = bf16[1536,2048]{1,0:T(8,128)(2,1)} fusion(bf16[129,2048]{1,0:T(8,128)(2,1)S(1)} %concatenate.11, s32[2048]{0:T(1024)S(1)} %pad_clamp_fusion), kind=kCustom, calls=%fused_computation | custom fusion | bytes 12589056 | tf_op jit(solution)/shard_map/gather | solution.py:83
  38.3 36.5 %all-to-all-done.1 = bf16[16,3,48,1,512]{4,2,3,1,0:T(8,128)(2,1)S(1)} async-done(((bf16[16,3,48,1,512]{4,2,3,1,0:T(8,128)(2,1)}), bf16[16,3,48,1,512]{4,2,3,1,0:T(8,128)(2,1)S(1)}, u32[]{:S(2)}, u32[]{:S(2)}) %all-to-all-start.1) | async-done | bytes 2359328 | tf_op jit(solution)/shard_map/all_to_all | solution.py:39
  74.8 0.2 copy.43
  74.9 6.5 %all_to_all.43 = bf16[2,3,384,1,512]{4,2,1,3,0:T(8,128)(2,1)} all-to-all(bf16[2,3,384,1,512]{4,2,1,3,0:T(8,128)(2,1)S(1)} %bitcast.99), channel_id=1, replica_groups=mesh['gr'=2,'fs'=8,'tp'=2] {'tp'}, dimensions={0} | all-to-all | bytes 4718592 | tf_op jit(solution)/shard_map/all_to_all | solution.py:38
  81.5 4.7 all-to-all-start
  86.2 0.0 all-gather.9.cloned.1.call-start
  86.2 0.7 all-gather.9.cloned.1.call-update
  86.9 65.5 %all-gather.9.cloned.1.call-done = bf16[1,3,384,4,1,512]{5,2,4,1,0,3:T(8,128)(2,1)} async-done(((bf16[1,3,384,2,1,512]{5,2,4,1,0,3:T(8,128)(2,1)}), bf16[1,3,384,4,1,512]{5,2,4,1,0,3:T(8,128)(2,1)}) %all-gather.9.cloned.1.call-update) | async-done | bytes 4718608 | tf_op jit(solution)/shard_map/all_gather | solution.py:45
  152.4 6.6 %copy.45 = bf16[1,3,384,4,1,512]{2,5,3,1,4,0:T(8,128)(2,1)} copy(bf16[1,3,384,4,1,512]{5,2,4,1,0,3:T(8,128)(2,1)} %all-gather.9.cloned.1.call-done) | data formatting | bytes 9437184 | tf_op jit(solution)/shard_map/all_gather | solution.py:45
  159.0 41.1 %all-to-all-done = bf16[16,96,2048]{2,1,0:T(8,128)(2,1)} async-done(((bf16[16,96,2048]{2,1,0:T(8,128)(2,1)}), bf16[16,96,2048]{2,1,0:T(8,128)(2,1)}, u32[]{:S(2)}, u32[]{:S(2)}) %all-to-all-start) | async-done | bytes 6291488 | tf_op jit(solution)/shard_map/all_to_all | solution.py:84
  200.2 5.9 %fusion.10 = f32[1536,384]{1,0:T(8,128)S(1)} fusion(bf16[1536,2048]{1,0:T(8,128)(2,1)} %bitcast.5, bf16[1,3,384,2048]{2,3,1,0:T(8,128)(2,1)} %bitcast.94), kind=kOutput, calls=%fused_computation.18 | convolution fusion | flops 2415919104 | bytes 10223616 | tf_op jit(solution)/shard_map/dot_general | solution.py:10
  206.1 11.4 %convolution_convert_fusion = bf16[1536,2048]{1,0:T(8,128)(2,1)} fusion(bf16[1,3,384,2048]{2,3,1,0:T(8,128)(2,1)} %bitcast.95, bf16[1536,2048]{1,0:T(8,128)(2,1)} %bitcast.5, f32[1536,384]{1,0:T(8,128)S(1)} %fusion.10), kind=kOutput, calls=%fused_computation.5 | convolution fusion | flops 4838522880 | bytes 18087936 | tf_op jit(solution)/shard_map/dot_general | solution.py:19
  217.5 28.2 %all-to-all-start.3 = ((bf16[16,96,2048]{2,1,0:T(8,128)(2,1)}), bf16[16,96,2048]{2,1,0:T(8,128)(2,1)}, u32[]{:S(2)}, u32[]{:S(2)}) async-start(bf16[16,96,2048]{2,1,0:T(8,128)(2,1)} %bitcast.100), calls=%async_computation.3 | async-start | bytes 12582912 | tf_op jit(solution)/shard_map/all_to_all | solution.py:90
  245.7 0.0 all-gather.11.cloned.1.call-start
  245.8 0.0 copy-done.4
  245.8 0.0 copy-done.2
  245.8 0.0 copy-done.3
  245.9 0.0 copy-start.7
  245.9 8.7 %all_gather.16 = bf16[3,64,2048]{2,1,0:T(8,128)(2,1)S(1)} all-gather(bf16[3,64,512]{2,1,0:T(8,128)(2,1)S(1)} %pad_maximum_fusion.1), channel_id=1, replica_groups=mesh['gr'=2,'fs'=8,'tp'=2] {'gr','tp'}, dimensions={2}, use_global_device_ids=true | all-gather | bytes 983040 | tf_op jit(solution)/shard_map/all_gather | solution.py:55
  254.6 1.2 slice_bitcast_fusion.3
  255.8 0.0 all-gather.11.cloned.1.call-update
  255.8 0.0 all-gather.13.cloned.1.call-start
  255.9 0.5 all-gather.13.cloned.1.call-update
  256.4 0.2 all-gather.15.cloned.1.call-start
  256.7 0.3 all-gather.15.cloned.1.call-update
  257.0 0.0 copy-done.7
  257.0 0.1 copy.46
  257.1 111.5 %all-gather.11.cloned.1.call-done = bf16[1,512,2048]{2,1,0:T(8,128)(2,1)} async-done(((bf16[1,64,2048]{2,1,0:T(8,128)(2,1)}), bf16[1,512,2048]{2,1,0:T(8,128)(2,1)}) %all-gather.11.cloned.1.call-update) | async-done | bytes 2097168 | tf_op jit(solution)/shard_map/all_gather | solution.py:67
  368.6 2.4 fusion.6
  371.0 4.5 slice_bitcast_fusion
  375.5 2.6 copy.47
  378.1 2.6 copy.48
  380.7 1.6 copy.49
  382.3 2.8 all-to-all-done.3
  385.1 12.4 %gather_fusion.1 = bf16[1024,2048]{1,0:T(8,128)(2,1)} fusion(bf16[1536,2048]{1,0:T(8,128)(2,1)} %bitcast.21, s32[1024]{0:T(1024)S(1)} %broadcast_clamp_fusion), kind=kCustom, calls=%fused_computation.1 | custom fusion | bytes 8392704 | tf_op jit(solution)/shard_map/gather | solution.py:91
  397.5 6.5 %fusion = f32[128,2048]{1,0:T(8,128)S(1)} fusion(bf16[1024,2048]{1,0:T(8,128)(2,1)} %gather_fusion.1, f32[128,8]{1,0:T(8,128)S(1)} %copy.46), kind=kLoop, calls=%fused_computation.4 | loop fusion | flops 6029312 | bytes 5246976 | tf_op jit(solution)/shard_map/reduce_sum | solution.py:93
  404.0 40.6 %all-gather.13.cloned.1.call-done = bf16[1,512,2048]{2,1,0:T(8,128)(2,1)} async-done(((bf16[1,64,2048]{2,1,0:T(8,128)(2,1)}), bf16[1,512,2048]{2,1,0:T(8,128)(2,1)}) %all-gather.13.cloned.1.call-update) | async-done | bytes 2097168 | tf_op jit(solution)/shard_map/all_gather | solution.py:68
  444.6 50.2 %all-gather.15.cloned.1.call-done = bf16[1,512,2048]{2,1,0:T(8,128)(2,1)} async-done(((bf16[1,64,2048]{2,1,0:T(8,128)(2,1)}), bf16[1,512,2048]{2,1,0:T(8,128)(2,1)}) %all-gather.15.cloned.1.call-update) | async-done | bytes 2097168 | tf_op jit(solution)/shard_map/all_gather | solution.py:69
  494.7 4.3 fusion.2
  (18 shorter events, 0.2 us)
Async XLA Ops:
  8.0 1.7 copy-start.6
  8.0 1.9 copy-start.1
  13.5 7.4 %copy-start.5 = (s32[128,8]{0,1:T(8,128)S(1)}, s32[128,8]{0,1:T(8,128)}, u32[]{:S(2)}) copy-start(s32[128,8]{0,1:T(8,128)} %param.11) | copy-start | bytes 12292
  13.5 12.8 %copy-start = (bf16[128,2048]{1,0:T(8,128)(2,1)S(1)}, bf16[128,2048]{1,0:T(8,128)(2,1)}, u32[]{:S(2)}) copy-start(bf16[128,2048]{1,0:T(8,128)(2,1)} %param.10) | copy-start | bytes 1572868
  13.5 61.3 %all-to-all-start.1 = ((bf16[16,3,48,1,512]{4,2,3,1,0:T(8,128)(2,1)}), bf16[16,3,48,1,512]{4,2,3,1,0:T(8,128)(2,1)S(1)}, u32[]{:S(2)}, u32[]{:S(2)}) async-start(bf16[16,3,48,1,512]{4,2,3,1,0:T(8,128)(2,1)} %pad_maximum_fusion), calls=%async_computation.1 | async-start | bytes 4718592 | tf_op jit(solution)/shard_map/all_to_all | solution.py:39
  81.5 118.7 %all-to-all-start = ((bf16[16,96,2048]{2,1,0:T(8,128)(2,1)}), bf16[16,96,2048]{2,1,0:T(8,128)(2,1)}, u32[]{:S(2)}, u32[]{:S(2)}) async-start(bf16[16,96,2048]{2,1,0:T(8,128)(2,1)} %bitcast.93), calls=%async_computation | async-start | bytes 12582912 | tf_op jit(solution)/shard_map/all_to_all | solution.py:84
  86.2 66.2 %all-gather.9.cloned.1.call-start = ((), (), s32[]{:S(2)}) async-start(), calls=%async_computation.4 | async-start | bytes 7077888 | tf_op jit(solution)/shard_map/all_gather | solution.py:45
  217.5 28.3 %copy-start.4 = (f32[64,512]{1,0:T(8,128)S(1)}, f32[64,512]{1,0:T(8,128)}, u32[]{:S(2)}) copy-start(f32[64,512]{1,0:T(8,128)} %param.19) | copy-start | bytes 393220
  217.5 28.3 %copy-start.2 = (f32[64,512]{1,0:T(8,128)S(1)}, f32[64,512]{1,0:T(8,128)}, u32[]{:S(2)}) copy-start(f32[64,512]{1,0:T(8,128)} %param.17) | copy-start | bytes 393220
  217.5 28.3 %copy-start.3 = (f32[64,512]{1,0:T(8,128)S(1)}, f32[64,512]{1,0:T(8,128)}, u32[]{:S(2)}) copy-start(f32[64,512]{1,0:T(8,128)} %param.18) | copy-start | bytes 393220
  217.5 167.6 %all-to-all-start.3 = ((bf16[16,96,2048]{2,1,0:T(8,128)(2,1)}), bf16[16,96,2048]{2,1,0:T(8,128)(2,1)}, u32[]{:S(2)}, u32[]{:S(2)}) async-start(bf16[16,96,2048]{2,1,0:T(8,128)(2,1)} %bitcast.100), calls=%async_computation.3 | async-start | bytes 12582912 | tf_op jit(solution)/shard_map/all_to_all | solution.py:90
  245.7 122.9 %all-gather.11.cloned.1.call-start = ((), (), s32[]{:S(2)}) async-start(), calls=%async_computation.5 | async-start | bytes 2359296 | tf_op jit(solution)/shard_map/all_gather | solution.py:67
  245.9 11.2 %copy-start.7 = (f32[128,8]{0,1:T(8,128)S(1)}, f32[128,8]{0,1:T(8,128)}, u32[]{:S(2)}) copy-start(f32[128,8]{0,1:T(8,128)} %param.12) | copy-start | bytes 12292
  255.8 188.7 %all-gather.13.cloned.1.call-start = ((), (), s32[]{:S(2)}) async-start(), calls=%async_computation.6 | async-start | bytes 2359296 | tf_op jit(solution)/shard_map/all_gather | solution.py:68
  256.4 238.3 %all-gather.15.cloned.1.call-start = ((), (), s32[]{:S(2)}) async-start(), calls=%async_computation.7 | async-start | bytes 2359296 | tf_op jit(solution)/shard_map/all_gather | solution.py:69
Sparse Core Ops, SparseCore 0:
  88.5 63.8 all-gather.8
Sparse Core Ops, SparseCore 1:
  255.9 112.6 all-gather.10
  370.6 73.9 all-gather.12
  447.1 47.5 all-gather.14
where the time goes:
time: 507 us
  waiting for transfers between devices  350 us (69%)
  local copies, waits for them, and re-layouts  44.2 us (9%)
  starting transfers between devices  40.7 us (8%)
  matrix products  24 us (5%)
  other arithmetic  16.8 us (3%)
  between operations  15.9 us (3%)
  blocking collectives  15.2 us (3%)
    all_gather x1, waiting for transfers between devices, body(): lax.all_gather(shared_gate, 'fs', axis=0, tiled=True)  111 us
    all_gather x1, waiting for transfers between devices, body(): owned = lax.all_gather(halves[:, :, :, None], 'gr', axis=3, tiled=True)  65.5 us
    all_gather x1, waiting for transfers between devices, body(): lax.all_gather(shared_down, 'fs', axis=0, tiled=True)  50.2 us
    all_to_all x1, waiting for transfers between devices, body(): lax.all_to_all(outgoing, ('fs', 'tp'), split_axis=0, concat_axis=0, tiled...  41.1 us
    all_gather x1, waiting for transfers between devices, body(): lax.all_gather(shared_up, 'fs', axis=0, tiled=True)  40.6 us
    all_to_all x1, waiting for transfers between devices, body(): lax.all_to_all(stacked[:, :, :, None, :], 'fs', split_axis=0, concat_axis...  36.5 us
    all_to_all x1, starting transfers between devices, body(): lax.all_to_all(result, ('fs', 'tp'), split_axis=0, concat_axis=0, tiled=T...  28.2 us
    dot_general x2, matrix products, swiglu_rows(): return jnp.dot(hidden, down_matrix, preferred_element_type=jnp.float32)  15.6 us
  transfers between devices with their start and end apart: 7, of which 7 were waited for; matrix products, arithmetic and copies ran while one was open for 11% of the time, Pallas kernels for 0%

commit v1 on v0

--- a/solution.py
+++ b/solution.py
@@ -35,13 +35,11 @@
     stacked = jnp.stack(
         [gate_trained * gain_row, up_trained * gain_row, down_trained], axis=1
     ).astype(jnp.bfloat16)
-    halves = lax.all_to_all(
-        lax.all_to_all(stacked[:, :, :, None, :], "fs", split_axis=0, concat_axis=2, tiled=True),
-        "tp",
-        split_axis=0,
-        concat_axis=3,
-        tiled=True,
-    )
+    part = lax.all_to_all(stacked[:, :, :, None, :], "fs", split_axis=0, concat_axis=2, tiled=True)
+    size = lax.axis_size("tp")
+    blocks = jnp.stack(jnp.split(part, size, axis=0), axis=0)
+    blocks = lax.all_to_all(blocks, "tp", split_axis=0, concat_axis=0)
+    halves = jnp.concatenate(blocks, axis=3)
     owned = lax.all_gather(halves[:, :, :, None], "gr", axis=3, tiled=True)
     owned = owned.reshape(owned.shape[0], 3, owned.shape[2], -1)
     expert_gate = owned[:, 0]

time: 507 us -> 508 us (level)
  no operation moved by 1% of the time
where the time goes in v1:
time: 508 us; the launch traced here: 507 us
  waiting for transfers between devices  350 us (69%)
  local copies, waits for them, and re-layouts  44.4 us (9%)
  starting transfers between devices  40.7 us (8%)
  matrix products  24 us (5%)
  other arithmetic  17 us (3%)
  between operations  15.9 us (3%)
  blocking collectives  15.3 us (3%)
    all_gather x1, waiting for transfers between devices, body(): lax.all_gather(shared_gate, 'fs', axis=0, tiled=True)  111 us
    all_gather x1, waiting for transfers between devices, body(): owned = lax.all_gather(halves[:, :, :, None], 'gr', axis=3, tiled=True)  65.5 us
    all_gather x1, waiting for transfers between devices, body(): lax.all_gather(shared_down, 'fs', axis=0, tiled=True)  50.2 us
    all_to_all x1, waiting for transfers between devices, body(): lax.all_to_all(outgoing, ('fs', 'tp'), split_axis=0, concat_axis=0, tiled...  41.1 us
    all_gather x1, waiting for transfers between devices, body(): lax.all_gather(shared_up, 'fs', axis=0, tiled=True)  40.6 us
    all_to_all x1, waiting for transfers between devices, body(): lax.all_to_all(stacked[:, :, :, None, :], 'fs', split_axis=0, concat_axis...  36.5 us
    all_to_all x1, starting transfers between devices, body(): lax.all_to_all(result, ('fs', 'tp'), split_axis=0, concat_axis=0, tiled=T...  28.2 us
    dot_general x2, matrix products, swiglu_rows(): return jnp.dot(hidden, down_matrix, preferred_element_type=jnp.float32)  15.6 us
  transfers between devices with their start and end apart: 7, of which 7 were waited for; matrix products, arithmetic and copies ran while one was open for 11% of the time, Pallas kernels for 0%

profile of v1, /device:TPU:0, one launch (start us, length us, event | category | flops | bytes accessed | tf_op | source)
XLA Modules:
  0.0 507.0 jit_solution(15531483860759654351)
XLA Ops:
  8.0 0.0 copy-start.6
  8.0 0.0 copy-start.1
  8.0 1.6 convert_bitcast_fusion
  9.7 0.0 copy-done.6
  9.7 0.2 copy-done.1
  9.9 1.9 fusion.27
  11.8 1.7 pad_maximum_fusion
  13.5 7.4 %all-to-all-start.1 = ((bf16[16,3,48,1,512]{4,2,1,3,0:T(8,128)(2,1)}), bf16[16,3,48,1,512]{4,2,1,3,0:T(8,128)(2,1)S(1)}, u32[]{:S(2)}, u32[]{:S(2)}) async-start(bf16[16,3,48,1,512]{4,2,1,3,0:T(8,128)(2,1)} %pad_maximum_fusion), calls=%async_computation.1 | async-start | bytes 4718592 | tf_op jit(solution)/shard_map/all_to_all | solution.py:38
  20.9 0.0 copy-done.5
  20.9 0.1 copy.40
  21.0 0.1 eq.29
  21.1 0.1 eq.25
  21.2 4.5 reduce-window.6
  25.8 0.1 slice.38
  25.8 0.1 copy.42
  26.0 0.1 copy.43
  26.1 0.1 copy.39
  26.2 0.1 mul.85
  26.3 0.0 copy-done
  26.3 0.2 fusion.23
  26.5 0.2 fusion.24
  26.7 0.1 broadcast_add_fusion
  26.9 4.3 scatter_custom_fusion
  31.2 7.1 %gather_fusion = bf16[1536,2048]{1,0:T(8,128)(2,1)} fusion(bf16[129,2048]{1,0:T(8,128)(2,1)S(1)} %concatenate.11, s32[2048]{0:T(1024)S(1)} %pad_clamp_fusion), kind=kCustom, calls=%fused_computation | custom fusion | bytes 12589056 | tf_op jit(solution)/shard_map/gather | solution.py:81
  38.3 36.5 %all-to-all-done.1 = bf16[16,3,48,1,512]{4,2,1,3,0:T(8,128)(2,1)S(1)} async-done(((bf16[16,3,48,1,512]{4,2,1,3,0:T(8,128)(2,1)}), bf16[16,3,48,1,512]{4,2,1,3,0:T(8,128)(2,1)S(1)}, u32[]{:S(2)}, u32[]{:S(2)}) %all-to-all-start.1) | async-done | bytes 2359328 | tf_op jit(solution)/shard_map/all_to_all | solution.py:38
  74.8 0.2 fusion.48
  75.0 0.1 copy.45
  75.1 0.1 copy.46
  75.2 0.2 pad_maximum_fusion.1
  75.4 6.5 %all_to_all.30 = bf16[2,1,3,384,1,512]{5,3,2,4,1,0:T(8,128)(2,1)} all-to-all(bf16[2,1,3,384,1,512]{5,3,2,4,1,0:T(8,128)(2,1)S(1)} %pad_maximum_fusion.1), channel_id=1, replica_groups=mesh['gr'=2,'fs'=8,'tp'=2] {'tp'}, dimensions={0} | all-to-all | bytes 4718592 | tf_op jit(solution)/shard_map/all_to_all | solution.py:41
  81.9 4.7 all-to-all-start
  86.6 0.0 all-gather.9.cloned.1.call-start
  86.6 0.7 all-gather.9.cloned.1.call-update
  87.3 65.5 %all-gather.9.cloned.1.call-done = bf16[1,3,384,4,1,512]{5,2,4,1,0,3:T(8,128)(2,1)} async-done(((bf16[1,3,384,2,1,512]{5,2,4,1,0,3:T(8,128)(2,1)}), bf16[1,3,384,4,1,512]{5,2,4,1,0,3:T(8,128)(2,1)}) %all-gather.9.cloned.1.call-update) | async-done | bytes 4718608 | tf_op jit(solution)/shard_map/all_gather | solution.py:43
  152.8 6.6 %copy.48 = bf16[1,3,384,4,1,512]{2,5,3,1,4,0:T(8,128)(2,1)} copy(bf16[1,3,384,4,1,512]{5,2,4,1,0,3:T(8,128)(2,1)} %all-gather.9.cloned.1.call-done) | data formatting | bytes 9437184 | tf_op jit(solution)/shard_map/all_gather | solution.py:43
  159.5 41.1 %all-to-all-done = bf16[16,96,2048]{2,1,0:T(8,128)(2,1)} async-done(((bf16[16,96,2048]{2,1,0:T(8,128)(2,1)}), bf16[16,96,2048]{2,1,0:T(8,128)(2,1)}, u32[]{:S(2)}, u32[]{:S(2)}) %all-to-all-start) | async-done | bytes 6291488 | tf_op jit(solution)/shard_map/all_to_all | solution.py:82
  200.6 5.9 %fusion.10 = f32[1536,384]{1,0:T(8,128)S(1)} fusion(bf16[1536,2048]{1,0:T(8,128)(2,1)} %bitcast.5, bf16[1,3,384,2048]{2,3,1,0:T(8,128)(2,1)} %bitcast.93), kind=kOutput, calls=%fused_computation.19 | convolution fusion | flops 2415919104 | bytes 10223616 | tf_op jit(solution)/shard_map/dot_general | solution.py:10
  206.5 11.4 %convolution_convert_fusion = bf16[1536,2048]{1,0:T(8,128)(2,1)} fusion(bf16[1,3,384,2048]{2,3,1,0:T(8,128)(2,1)} %bitcast.94, bf16[1536,2048]{1,0:T(8,128)(2,1)} %bitcast.5, f32[1536,384]{1,0:T(8,128)S(1)} %fusion.10), kind=kOutput, calls=%fused_computation.5 | convolution fusion | flops 4838522880 | bytes 18087936 | tf_op jit(solution)/shard_map/dot_general | solution.py:19
  217.9 28.2 %all-to-all-start.3 = ((bf16[16,96,2048]{2,1,0:T(8,128)(2,1)}), bf16[16,96,2048]{2,1,0:T(8,128)(2,1)}, u32[]{:S(2)}, u32[]{:S(2)}) async-start(bf16[16,96,2048]{2,1,0:T(8,128)(2,1)} %bitcast.98), calls=%async_computation.3 | async-start | bytes 12582912 | tf_op jit(solution)/shard_map/all_to_all | solution.py:88
  246.2 0.0 all-gather.11.cloned.1.call-start
  246.2 0.0 copy-done.4
  246.2 0.0 copy-done.2
  246.3 0.0 copy-done.3
  246.3 0.0 copy-start.7
  246.3 8.7 %all_gather.16 = bf16[3,64,2048]{2,1,0:T(8,128)(2,1)S(1)} all-gather(bf16[3,64,512]{2,1,0:T(8,128)(2,1)S(1)} %pad_maximum_fusion.2), channel_id=1, replica_groups=mesh['gr'=2,'fs'=8,'tp'=2] {'gr','tp'}, dimensions={2}, use_global_device_ids=true | all-gather | bytes 983040 | tf_op jit(solution)/shard_map/all_gather | solution.py:53
  255.1 1.2 slice_bitcast_fusion.3
  256.3 0.0 all-gather.11.cloned.1.call-update
  256.3 0.0 all-gather.13.cloned.1.call-start
  256.3 0.5 all-gather.13.cloned.1.call-update
  256.9 0.2 all-gather.15.cloned.1.call-start
  257.1 0.3 all-gather.15.cloned.1.call-update
  257.5 0.1 copy.49
  257.6 111.5 %all-gather.11.cloned.1.call-done = bf16[1,512,2048]{2,1,0:T(8,128)(2,1)} async-done(((bf16[1,64,2048]{2,1,0:T(8,128)(2,1)}), bf16[1,512,2048]{2,1,0:T(8,128)(2,1)}) %all-gather.11.cloned.1.call-update) | async-done | bytes 2097168 | tf_op jit(solution)/shard_map/all_gather | solution.py:65
  369.0 2.4 fusion.6
  371.5 4.5 slice_bitcast_fusion
  376.0 2.6 copy.50
  378.5 2.6 copy.51
  381.1 1.6 copy.52
  382.7 2.8 all-to-all-done.3
  385.5 12.4 %gather_fusion.1 = bf16[1024,2048]{1,0:T(8,128)(2,1)} fusion(bf16[1536,2048]{1,0:T(8,128)(2,1)} %bitcast.22, s32[1024]{0:T(1024)S(1)} %broadcast_clamp_fusion), kind=kCustom, calls=%fused_computation.1 | custom fusion | bytes 8392704 | tf_op jit(solution)/shard_map/gather | solution.py:89
  397.9 6.5 %fusion = f32[128,2048]{1,0:T(8,128)S(1)} fusion(bf16[1024,2048]{1,0:T(8,128)(2,1)} %gather_fusion.1, f32[128,8]{1,0:T(8,128)S(1)} %copy.49), kind=kLoop, calls=%fused_computation.4 | loop fusion | flops 6029312 | bytes 5246976 | tf_op jit(solution)/shard_map/reduce_sum | solution.py:91
  404.4 40.6 %all-gather.13.cloned.1.call-done = bf16[1,512,2048]{2,1,0:T(8,128)(2,1)} async-done(((bf16[1,64,2048]{2,1,0:T(8,128)(2,1)}), bf16[1,512,2048]{2,1,0:T(8,128)(2,1)}) %all-gather.13.cloned.1.call-update) | async-done | bytes 2097168 | tf_op jit(solution)/shard_map/all_gather | solution.py:66
  445.0 50.2 %all-gather.15.cloned.1.call-done = bf16[1,512,2048]{2,1,0:T(8,128)(2,1)} async-done(((bf16[1,64,2048]{2,1,0:T(8,128)(2,1)}), bf16[1,512,2048]{2,1,0:T(8,128)(2,1)}) %all-gather.15.cloned.1.call-update) | async-done | bytes 2097168 | tf_op jit(solution)/shard_map/all_gather | solution.py:67
  495.2 4.3 fusion.2
  (21 shorter events, 0.2 us)
Async XLA Ops:
  8.0 1.7 copy-start.6
  8.0 1.9 copy-start.1
  13.5 7.4 %copy-start.5 = (s32[128,8]{0,1:T(8,128)S(1)}, s32[128,8]{0,1:T(8,128)}, u32[]{:S(2)}) copy-start(s32[128,8]{0,1:T(8,128)} %param.11) | copy-start | bytes 12292
  13.5 12.8 %copy-start = (bf16[128,2048]{1,0:T(8,128)(2,1)S(1)}, bf16[128,2048]{1,0:T(8,128)(2,1)}, u32[]{:S(2)}) copy-start(bf16[128,2048]{1,0:T(8,128)(2,1)} %param.10) | copy-start | bytes 1572868
  13.5 61.3 %all-to-all-start.1 = ((bf16[16,3,48,1,512]{4,2,1,3,0:T(8,128)(2,1)}), bf16[16,3,48,1,512]{4,2,1,3,0:T(8,128)(2,1)S(1)}, u32[]{:S(2)}, u32[]{:S(2)}) async-start(bf16[16,3,48,1,512]{4,2,1,3,0:T(8,128)(2,1)} %pad_maximum_fusion), calls=%async_computation.1 | async-start | bytes 4718592 | tf_op jit(solution)/shard_map/all_to_all | solution.py:38
  81.9 118.7 %all-to-all-start = ((bf16[16,96,2048]{2,1,0:T(8,128)(2,1)}), bf16[16,96,2048]{2,1,0:T(8,128)(2,1)}, u32[]{:S(2)}, u32[]{:S(2)}) async-start(bf16[16,96,2048]{2,1,0:T(8,128)(2,1)} %bitcast.92), calls=%async_computation | async-start | bytes 12582912 | tf_op jit(solution)/shard_map/all_to_all | solution.py:82
  86.6 66.2 %all-gather.9.cloned.1.call-start = ((), (), s32[]{:S(2)}) async-start(), calls=%async_computation.4 | async-start | bytes 7077888 | tf_op jit(solution)/shard_map/all_gather | solution.py:43
  217.9 28.3 %copy-start.4 = (f32[64,512]{1,0:T(8,128)S(1)}, f32[64,512]{1,0:T(8,128)}, u32[]{:S(2)}) copy-start(f32[64,512]{1,0:T(8,128)} %param.19) | copy-start | bytes 393220
  217.9 28.3 %copy-start.2 = (f32[64,512]{1,0:T(8,128)S(1)}, f32[64,512]{1,0:T(8,128)}, u32[]{:S(2)}) copy-start(f32[64,512]{1,0:T(8,128)} %param.17) | copy-start | bytes 393220
  217.9 28.3 %copy-start.3 = (f32[64,512]{1,0:T(8,128)S(1)}, f32[64,512]{1,0:T(8,128)}, u32[]{:S(2)}) copy-start(f32[64,512]{1,0:T(8,128)} %param.18) | copy-start | bytes 393220
  217.9 167.6 %all-to-all-start.3 = ((bf16[16,96,2048]{2,1,0:T(8,128)(2,1)}), bf16[16,96,2048]{2,1,0:T(8,128)(2,1)}, u32[]{:S(2)}, u32[]{:S(2)}) async-start(bf16[16,96,2048]{2,1,0:T(8,128)(2,1)} %bitcast.98), calls=%async_computation.3 | async-start | bytes 12582912 | tf_op jit(solution)/shard_map/all_to_all | solution.py:88
  246.2 122.9 %all-gather.11.cloned.1.call-start = ((), (), s32[]{:S(2)}) async-start(), calls=%async_computation.5 | async-start | bytes 2359296 | tf_op jit(solution)/shard_map/all_gather | solution.py:65
  246.3 11.2 %copy-start.7 = (f32[128,8]{0,1:T(8,128)S(1)}, f32[128,8]{0,1:T(8,128)}, u32[]{:S(2)}) copy-start(f32[128,8]{0,1:T(8,128)} %param.12) | copy-start | bytes 12292
  256.3 188.7 %all-gather.13.cloned.1.call-start = ((), (), s32[]{:S(2)}) async-start(), calls=%async_computation.6 | async-start | bytes 2359296 | tf_op jit(solution)/shard_map/all_gather | solution.py:66
  256.9 238.3 %all-gather.15.cloned.1.call-start = ((), (), s32[]{:S(2)}) async-start(), calls=%async_computation.7 | async-start | bytes 2359296 | tf_op jit(solution)/shard_map/all_gather | solution.py:67
Sparse Core Ops, SparseCore 0:
  88.9 63.8 all-gather.8
Sparse Core Ops, SparseCore 1:
  256.4 112.6 all-gather.10
  371.0 73.9 all-gather.12
  447.6 47.5 all-gather.14
